TPU v7x, 32 devices: a whole 2x2x4 slice. The times are simulated.
32 devices in a mesh: gr: 2 (over x), fs: 8 (over z, y), tp: 2 (over core).
Axes of the slice: x: 2, y: 2, z: 4, core: 2. Of those that a mesh axis runs over, the one named last changes fastest.
Arguments:
- tokens: bfloat16 [4, 2048, 2048], P(('gr', 'tp')), may hold values from -6 to 6
- gate_master: float32 [3, 2048, 7168], P(None, 'fs', ('gr', 'tp')), may hold values from -0.125 to 0.125
- up_master: float32 [3, 2048, 7168], P(None, 'fs', ('gr', 'tp')), may hold values from -0.125 to 0.125
- down_master: float32 [3, 7168, 2048], P(None, 'fs', ('gr', 'tp')), may hold values from -0.0625 to 0.0625
- norm_gain: float32 [2048], P('fs'), may hold values from 0.1 to 1.9
- route: int32 [4, 2048, 2], P(('gr', 'tp')), may hold values from 0 to 2, all different within a row
- route_weight: float32 [4, 2048, 2], P(('gr', 'tp')), may hold values from 0.05 to 1
Outputs:
- gate_out: bfloat16 [3, 2048, 7168], P(None, None, 'fs')
- up_out: bfloat16 [3, 2048, 7168], P(None, None, 'fs')
- down_out: bfloat16 [3, 7168, 2048], P(None, 'fs')
- mixed: bfloat16 [4, 2048, 2048], P(('gr', 'tp'), 'fs')
Inputs may be any that keep to these rules, and one draw needn't show every extreme that they name: `route`: each token names two different experts; every expert is named by some token.
All inputs are finite; a program needn't handle non-finite values.
Results may differ from a plain program's by a relative error of at most 0.024.
Values may be sent and summed in bfloat16 or wider, within the bound.
A program may use at most 192 MiB of HBM per device.

v0:
```python
import jax
import jax.numpy as jnp
from jax import lax
from jax.sharding import PartitionSpec as P


def normalize(rows_in):
    values = rows_in.astype(jnp.float32)
    scaled = values * lax.rsqrt(jnp.mean(values * values, axis=-1, keepdims=True) + 1e-06)
    return scaled.astype(jnp.bfloat16)


def mixing(chosen, weights, experts):
    share = weights / jnp.sum(weights, axis=-1, keepdims=True)
    labels = jnp.arange(experts, dtype=jnp.int32)
    match = (chosen[:, :, None] == labels[None, None, :]).astype(jnp.float32)
    return jnp.sum(share[:, :, None] * match, axis=1)


def expert_term(normed, mix_column, gate_weight, up_weight, down_weight):
    gate_act = jnp.dot(normed, gate_weight, preferred_element_type=jnp.float32)
    up_act = jnp.dot(normed, up_weight, preferred_element_type=jnp.float32)
    hidden = (jax.nn.silu(gate_act) * up_act).astype(jnp.bfloat16)
    projected = jnp.dot(hidden, down_weight, preferred_element_type=jnp.float32)
    return mix_column * projected


def shards(tokens, gate_master, up_master, down_master, norm_gain, route, route_weight):
    scaled_gain = norm_gain[None, :, None]
    gate_local = (scaled_gain * gate_master).astype(jnp.bfloat16)
    up_local = (scaled_gain * up_master).astype(jnp.bfloat16)
    down_local = down_master.astype(jnp.bfloat16)
    experts = gate_local.shape[0]
    normed = normalize(tokens[0])
    combine = mixing(route[0], route_weight[0], experts)
    width = normed.shape[1]
    gate_list = []
    up_list = []
    down_list = []
    total = jnp.zeros((normed.shape[0], width), jnp.float32)
    for index in range(experts):
        gate_rows, up_rows, down_full = (
            lax.all_gather(gate_local[index], ("gr", "tp"), axis=1, tiled=True),
            lax.all_gather(up_local[index], ("gr", "tp"), axis=1, tiled=True),
            lax.all_gather(down_local[index], ("gr", "tp"), axis=1, tiled=True),
        )
        gate_block, up_block = (
            lax.all_to_all(gate_rows, "fs", split_axis=1, concat_axis=0, tiled=True),
            lax.all_to_all(up_rows, "fs", split_axis=1, concat_axis=0, tiled=True),
        )
        total = total + expert_term(
            normed, combine[:, index : index + 1], gate_block, up_block, down_full
        )
        gate_list.append(gate_block)
        up_list.append(up_block)
        down_list.append(down_full)
    gate_out = jnp.stack(gate_list, axis=0)
    up_out = jnp.stack(up_list, axis=0)
    down_out = jnp.stack(down_list, axis=0)
    summed = lax.psum_scatter(total.astype(jnp.bfloat16), "fs", scatter_dimension=0, tiled=True)
    mixed = summed[None]
    return (gate_out, up_out, down_out, mixed)


def solution(mesh):
    in_specs = (
        P(("gr", "tp"), None, None),
        P(None, "fs", ("gr", "tp")),
        P(None, "fs", ("gr", "tp")),
        P(None, "fs", ("gr", "tp")),
        P("fs"),
        P(("gr", "tp"), None, None),
        P(("gr", "tp"), None, None),
    )
    out_specs = (
        P(None, None, "fs"),
        P(None, None, "fs"),
        P(None, "fs", None),
        P(("gr", "tp"), "fs", None),
    )
    return jax.shard_map(shards, mesh=mesh, in_specs=in_specs, out_specs=out_specs, check_vma=False)
```

profile of v0, /device:TPU:0, one launch (start us, length us, event | category | flops | bytes accessed | tf_op | source)
XLA Modules:
  0.0 764.3 jit_solution(10125969847166633548)
XLA Ops:
  7.2 5.2 multiply_convert_fusion.3
  17.0 31.4 %all-gather.21.cloned.1.call-done = bf16[1,256,7168]{2,1,0:T(8,128)(2,1)} async-done(((bf16[1,256,1792]{2,1,0:T(8,128)(2,1)}), bf16[1,256,7168]{2,1,0:T(8,128)(2,1)}) %all-gather.21.cloned.1.call-update) | async-done | bytes 3670032 | tf_op jit(solution)/shard_map/all_gather | solution.py:43
  48.4 2.8 copy.34
  53.6 5.5 all-to-all-start.1
  59.7 22.3 %all-gather.27.cloned.1.call-done = bf16[1,256,7168]{2,1,0:T(8,128)(2,1)} async-done(((bf16[1,256,1792]{2,1,0:T(8,128)(2,1)}), bf16[1,256,7168]{2,1,0:T(8,128)(2,1)}) %all-gather.27.cloned.1.call-update) | async-done | bytes 3670032 | tf_op jit(solution)/shard_map/all_gather | solution.py:44
  87.3 54.3 %all-to-all-done.1 = bf16[256,8,896]{2,0,1:T(8,128)(2,1)} async-done(((bf16[256,8,896]{2,0,1:T(8,128)(2,1)}), bf16[256,8,896]{2,0,1:T(8,128)(2,1)}, u32[]{:S(2)}, u32[]{:S(2)}) %all-to-all-start.1) | async-done | bytes 3670048 | tf_op jit(solution)/shard_map/all_to_all | solution.py:48
  141.6 4.5 all-to-all-start.4
  146.7 2.8 copy.33
  151.9 75.7 %all-to-all-done.4 = bf16[256,8,896]{2,0,1:T(8,128)(2,1)} async-done(((bf16[256,8,896]{2,0,1:T(8,128)(2,1)}), bf16[256,8,896]{2,0,1:T(8,128)(2,1)}, u32[]{:S(2)}, u32[]{:S(2)}) %all-to-all-start.4) | async-done | bytes 3670048 | tf_op jit(solution)/shard_map/all_to_all | solution.py:49
  227.6 4.5 all-to-all-start
  232.2 2.9 convert_element_type.45
  237.5 2.8 copy.36
  242.7 70.7 %all-to-all-done = bf16[256,8,896]{2,0,1:T(8,128)(2,1)} async-done(((bf16[256,8,896]{2,0,1:T(8,128)(2,1)}), bf16[256,8,896]{2,0,1:T(8,128)(2,1)}, u32[]{:S(2)}, u32[]{:S(2)}) %all-to-all-start) | async-done | bytes 3670048 | tf_op jit(solution)/shard_map/all_to_all | solution.py:48
  313.5 4.5 all-to-all-start.3
  318.9 5.1 fusion
  324.0 2.8 copy.35
  329.2 70.1 %all-to-all-done.3 = bf16[256,8,896]{2,0,1:T(8,128)(2,1)} async-done(((bf16[256,8,896]{2,0,1:T(8,128)(2,1)}), bf16[256,8,896]{2,0,1:T(8,128)(2,1)}, u32[]{:S(2)}, u32[]{:S(2)}) %all-to-all-start.3) | async-done | bytes 3670048 | tf_op jit(solution)/shard_map/all_to_all | solution.py:49
  399.3 16.6 %all-to-all-start.2 = ((bf16[256,8,896]{2,0,1:T(8,128)(2,1)}), bf16[256,8,896]{2,0,1:T(8,128)(2,1)}, u32[]{:S(2)}, u32[]{:S(2)}) async-start(bf16[256,8,896]{2,0,1:T(8,128)(2,1)} %copy.29), calls=%async_computation.2 | async-start | bytes 7340032 | tf_op jit(solution)/shard_map/all_to_all | solution.py:48
  416.0 2.8 copy.38
  421.2 14.2 %fusion.21 = f32[2048,896]{1,0:T(8,128)} fusion(bf16[2048,896]{1,0:T(8,128)(2,1)} %bitcast.20, bf16[1,2048,2048]{2,1,0:T(8,128)(2,1)} %param.7, f32[2048]{0:T(1024)S(1)} %add_rsqrt_fusion), kind=kOutput, calls=%fused_computation.30 | convolution fusion | flops 7528775680 | bytes 19406848 | tf_op jit(solution)/shard_map/dot_general | solution.py:21
  435.5 26.7 %fusion.3 = f32[2048,2048]{1,0:T(8,128)} fusion(f32[2048,896]{1,0:T(8,128)} %fusion.21, bf16[2048,896]{1,0:T(8,128)(2,1)} %bitcast.21, bf16[1,896,2048]{2,1,0:T(8,128)(2,1)} %all-gather.33.cloned.1.call-done, bf16[1,2048,2048]{2,1,0:T(8,128)(2,1)} %param.7, f32[2048]{0:T(1024)S(1)} %add_rsqrt_fusion), kind=kOutput, calls=%fused_computation.14 | convolution fusion | flops 15055978496 | bytes 39854080 | tf_op jit(solution)/shard_map/dot_general | solution.py:24
  462.2 35.0 %all-to-all-done.2 = bf16[256,8,896]{2,0,1:T(8,128)(2,1)} async-done(((bf16[256,8,896]{2,0,1:T(8,128)(2,1)}), bf16[256,8,896]{2,0,1:T(8,128)(2,1)}, u32[]{:S(2)}, u32[]{:S(2)}) %all-to-all-start.2) | async-done | bytes 3670048 | tf_op jit(solution)/shard_map/all_to_all | solution.py:48
  497.2 4.5 all-to-all-start.5
  501.8 14.2 %fusion.25 = f32[2048,896]{1,0:T(8,128)} fusion(bf16[2048,896]{1,0:T(8,128)(2,1)} %bitcast.16, bf16[1,2048,2048]{2,1,0:T(8,128)(2,1)} %param.7, f32[2048]{0:T(1024)S(1)} %add_rsqrt_fusion), kind=kOutput, calls=%fused_computation.31 | convolution fusion | flops 7528775680 | bytes 19406848 | tf_op jit(solution)/shard_map/dot_general | solution.py:21
  516.0 14.2 %fusion.17 = f32[2048,896]{1,0:T(8,128)} fusion(bf16[2048,896]{1,0:T(8,128)(2,1)} %bitcast.24, bf16[1,2048,2048]{2,1,0:T(8,128)(2,1)} %param.7, f32[2048]{0:T(1024)S(1)} %add_rsqrt_fusion), kind=kOutput, calls=%fused_computation.29 | convolution fusion | flops 7528775680 | bytes 19406848 | tf_op jit(solution)/shard_map/dot_general | solution.py:21
  530.2 26.9 %fusion.4 = f32[2048,2048]{1,0:T(8,128)} fusion(f32[2048,896]{1,0:T(8,128)} %fusion.25, bf16[2048,896]{1,0:T(8,128)(2,1)} %bitcast.17, bf16[1,896,2048]{2,1,0:T(8,128)(2,1)} %all-gather.31.cloned.1.call-done, bf16[1,2048,2048]{2,1,0:T(8,128)(2,1)} %param.7, f32[2048]{0:T(1024)S(1)} %add_rsqrt_fusion), kind=kOutput, calls=%fused_computation.15 | convolution fusion | flops 15055978496 | bytes 39854080 | tf_op jit(solution)/shard_map/dot_general | solution.py:24
  557.1 25.8 %all-to-all-done.5 = bf16[256,8,896]{2,0,1:T(8,128)(2,1)} async-done(((bf16[256,8,896]{2,0,1:T(8,128)(2,1)}), bf16[256,8,896]{2,0,1:T(8,128)(2,1)}, u32[]{:S(2)}, u32[]{:S(2)}) %all-to-all-start.5) | async-done | bytes 3670048 | tf_op jit(solution)/shard_map/all_to_all | solution.py:49
  582.9 28.4 %add_convert_fusion = bf16[2048,2048]{1,0:T(8,128)(2,1)} fusion(f32[2048,2048]{1,0:T(8,128)} %fusion.3, f32[2048,2048]{1,0:T(8,128)} %fusion.4, f32[2048]{0:T(1024)S(1)} %bitcast.95, f32[2048]{0:T(1024)S(1)} %bitcast.96, f32[2048]{0:T(1024)S(1)} %bitcast.94, f32[2048,896]{1,0:T(8,128)} %fusion.17, bf16[2048,896]{1,0:T(8,128)(2,1)} %bitcast.25, ...), kind=kOutput, calls=%fused_computation.4 | convolution fusion | flops 15081144320 | bytes 65044480 | tf_op jit(solution)/shard_map/dot_general | solution.py:24
  611.3 9.8 %pad_maximum_fusion.2 = bf16[3,896,2048]{2,1,0:T(8,128)(2,1)} fusion(bf16[1,896,2048]{2,1,0:T(8,128)(2,1)} %all-gather.35.cloned.1.call-done, bf16[1,896,2048]{2,1,0:T(8,128)(2,1)} %all-gather.33.cloned.1.call-done, bf16[1,896,2048]{2,1,0:T(8,128)(2,1)} %all-gather.31.cloned.1.call-done), kind=kLoop, calls=%fused_computation.7 | loop fusion | flops 11010048 | bytes 22020096 | tf_op jit(solution)/shard_map/stack | solution.py:59
  621.1 9.8 %pad_maximum_fusion.1 = bf16[3,2048,896]{2,1,0:T(8,128)(2,1)} fusion(bf16[1,2048,896]{2,1,0:T(8,128)(2,1)} %bitcast.11, bf16[1,2048,896]{2,1,0:T(8,128)(2,1)} %bitcast.9, bf16[1,2048,896]{2,1,0:T(8,128)(2,1)} %bitcast.7), kind=kLoop, calls=%fused_computation.6 | loop fusion | flops 11010048 | bytes 22020096 | tf_op jit(solution)/shard_map/stack | solution.py:58
  630.9 9.8 %pad_maximum_fusion = bf16[3,2048,896]{2,1,0:T(8,128)(2,1)} fusion(bf16[1,2048,896]{2,1,0:T(8,128)(2,1)} %bitcast.5, bf16[1,2048,896]{2,1,0:T(8,128)(2,1)} %bitcast.3, bf16[1,2048,896]{2,1,0:T(8,128)(2,1)} %bitcast.1), kind=kLoop, calls=%fused_computation.5 | loop fusion | flops 11010048 | bytes 22020096 | tf_op jit(solution)/shard_map/stack | solution.py:57
  640.6 116.5 %reduce-scatter.2.cloned.1.call-done = bf16[256,2048]{1,0:T(8,128)(2,1)} async-done(((bf16[2048,2048]{1,0:T(8,128)(2,1)}), bf16[256,2048]{1,0:T(8,128)(2,1)}) %reduce-scatter.2.cloned.1.call-update) | async-done | bytes 1048592 | tf_op jit(solution)/shard_map/reduce_scatter | solution.py:60
  (46 shorter events, 26.5 us)
Async XLA Ops:
  7.2 41.2 %all-gather.21.cloned.1.call-start = ((), (), s32[]{:S(2)}) async-start(), calls=%async_computation.9 | async-start | bytes 4587520 | tf_op jit(solution)/shard_map/all_gather | solution.py:43
  14.0 68.0 %all-gather.27.cloned.1.call-start = ((), (), s32[]{:S(2)}) async-start(), calls=%async_computation.12 | async-start | bytes 4587520 | tf_op jit(solution)/shard_map/all_gather | solution.py:44
  15.7 131.0 %all-gather.19.cloned.1.call-start = ((), (), s32[]{:S(2)}) async-start(), calls=%async_computation.8 | async-start | bytes 4587520 | tf_op jit(solution)/shard_map/all_gather | solution.py:43
  16.4 221.1 %all-gather.25.cloned.1.call-start = ((), (), s32[]{:S(2)}) async-start(), calls=%async_computation.11 | async-start | bytes 4587520 | tf_op jit(solution)/shard_map/all_gather | solution.py:44
  53.6 88.0 %all-to-all-start.1 = ((bf16[256,8,896]{2,0,1:T(8,128)(2,1)}), bf16[256,8,896]{2,0,1:T(8,128)(2,1)}, u32[]{:S(2)}, u32[]{:S(2)}) async-start(bf16[256,8,896]{2,0,1:T(8,128)(2,1)} %copy.28), calls=%async_computation.1 | async-start | bytes 7340032 | tf_op jit(solution)/shard_map/all_to_all | solution.py:48
  59.1 264.9 %all-gather.23.cloned.1.call-start = ((), (), s32[]{:S(2)}) async-start(), calls=%async_computation.10 | async-start | bytes 4587520 | tf_op jit(solution)/shard_map/all_gather | solution.py:43
  141.6 86.0 %all-to-all-start.4 = ((bf16[256,8,896]{2,0,1:T(8,128)(2,1)}), bf16[256,8,896]{2,0,1:T(8,128)(2,1)}, u32[]{:S(2)}, u32[]{:S(2)}) async-start(bf16[256,8,896]{2,0,1:T(8,128)(2,1)} %copy.31), calls=%async_computation.4 | async-start | bytes 7340032 | tf_op jit(solution)/shard_map/all_to_all | solution.py:49
  146.1 269.9 %all-gather.29.cloned.1.call-start = ((), (), s32[]{:S(2)}) async-start(), calls=%async_computation.13 | async-start | bytes 4587520 | tf_op jit(solution)/shard_map/all_gather | solution.py:44
  227.6 85.9 %all-to-all-start = ((bf16[256,8,896]{2,0,1:T(8,128)(2,1)}), bf16[256,8,896]{2,0,1:T(8,128)(2,1)}, u32[]{:S(2)}, u32[]{:S(2)}) async-start(bf16[256,8,896]{2,0,1:T(8,128)(2,1)} %copy.27), calls=%async_computation | async-start | bytes 7340032 | tf_op jit(solution)/shard_map/all_to_all | solution.py:48
  232.1 203.3 %all-gather.33.cloned.1.call-start = ((), (), s32[]{:S(2)}) async-start(), calls=%async_computation.15 | async-start | bytes 4587520 | tf_op jit(solution)/shard_map/all_gather | solution.py:45
  236.7 293.5 %all-gather.31.cloned.1.call-start = ((), (), s32[]{:S(2)}) async-start(), calls=%async_computation.14 | async-start | bytes 4587520 | tf_op jit(solution)/shard_map/all_gather | solution.py:45
  240.3 78.5 %copy-start = (f32[1,2048,2]{1,2,0:T(2,128)S(1)}, f32[1,2048,2]{1,2,0:T(2,128)}, u32[]{:S(2)}) copy-start(f32[1,2048,2]{1,2,0:T(2,128)} %param.13) | copy-start | bytes 49156
  240.3 78.5 %copy-start.1 = (s32[1,2048,2]{1,2,0:T(2,128)S(1)}, s32[1,2048,2]{1,2,0:T(2,128)}, u32[]{:S(2)}) copy-start(s32[1,2048,2]{1,2,0:T(2,128)} %param.12) | copy-start | bytes 49156
  313.5 85.9 %all-to-all-start.3 = ((bf16[256,8,896]{2,0,1:T(8,128)(2,1)}), bf16[256,8,896]{2,0,1:T(8,128)(2,1)}, u32[]{:S(2)}, u32[]{:S(2)}) async-start(bf16[256,8,896]{2,0,1:T(8,128)(2,1)} %copy.30), calls=%async_computation.3 | async-start | bytes 7340032 | tf_op jit(solution)/shard_map/all_to_all | solution.py:49
  318.0 239.1 %all-gather.35.cloned.1.call-start = ((), (), s32[]{:S(2)}) async-start(), calls=%async_computation.16 | async-start | bytes 4587520 | tf_op jit(solution)/shard_map/all_gather | solution.py:45
  399.3 97.9 %all-to-all-start.2 = ((bf16[256,8,896]{2,0,1:T(8,128)(2,1)}), bf16[256,8,896]{2,0,1:T(8,128)(2,1)}, u32[]{:S(2)}, u32[]{:S(2)}) async-start(bf16[256,8,896]{2,0,1:T(8,128)(2,1)} %copy.29), calls=%async_computation.2 | async-start | bytes 7340032 | tf_op jit(solution)/shard_map/all_to_all | solution.py:48
  497.2 85.7 %all-to-all-start.5 = ((bf16[256,8,896]{2,0,1:T(8,128)(2,1)}), bf16[256,8,896]{2,0,1:T(8,128)(2,1)}, u32[]{:S(2)}, u32[]{:S(2)}) async-start(bf16[256,8,896]{2,0,1:T(8,128)(2,1)} %copy.32), calls=%async_computation.5 | async-start | bytes 7340032 | tf_op jit(solution)/shard_map/all_to_all | solution.py:49
  501.7 255.4 %reduce-scatter.2.cloned.1.call-start = ((), (), s32[]{:S(2)}) async-start(), calls=%async_computation.7 | async-start | bytes 9437184 | tf_op jit(solution)/shard_map/reduce_scatter | solution.py:60
Sparse Core Ops, SparseCore 0:
  14.1 34.1 all-gather.20
  50.5 31.4 all-gather.26
  84.2 31.4 all-gather.18
  117.7 31.4 all-gather.24
  150.6 31.4 all-gather.22
  183.5 31.4 all-gather.28
  236.8 31.8 all-gather.32
  270.8 31.4 all-gather.30
  320.4 31.8 all-gather.34
  611.5 145.5 reduce-scatter.1
where the time goes:
time: 767 us; the launch traced here: 764 us
  waiting for transfers between devices  506 us (66%)
  matrix products  125 us (16%)
  other arithmetic  42.6 us (6%)
  starting transfers between devices  40.6 us (5%)
  local copies, waits for them, and re-layouts  36.1 us (5%)
  between operations  14.8 us (2%)
    all_to_all x3, waiting for transfers between devices, shards(): lax.all_to_all(up_rows, 'fs', split_axis=1, concat_axis=0, tiled=True)  172 us
    all_to_all x3, waiting for transfers between devices, shards(): lax.all_to_all(gate_rows, 'fs', split_axis=1, concat_axis=0, tiled=True)  160 us
    reduce_scatter x1, waiting for transfers between devices, shards(): lax.psum_scatter(total.astype(jnp.bfloat16), 'fs', scatter_dimension=0, t...  116 us
    dot_general x3, matrix products, expert_term(): projected = jnp.dot(hidden, down_weight, preferred_element_type=jnp.float32)  82 us
    dot_general x3, matrix products, expert_term(): gate_act = jnp.dot(normed, gate_weight, preferred_element_type=jnp.float32)  42.7 us
    all_gather x3, waiting for transfers between devices, shards(): lax.all_gather(gate_local[index], ('gr', 'tp'), axis=1, tiled=True)  31.4 us
    all_to_all x3, starting transfers between devices, shards(): lax.all_to_all(gate_rows, 'fs', split_axis=1, concat_axis=0, tiled=True)  26.6 us
    all_gather x3, waiting for transfers between devices, shards(): lax.all_gather(up_local[index], ('gr', 'tp'), axis=1, tiled=True)  22.4 us
  transfers between devices with their start and end apart: 16, of which 9 were waited for; matrix products, arithmetic and copies ran while one was open for 22% of the time, Pallas kernels for 0%

commit v1 on v0

v1 whole, which is shorter than its diff:
```python
import jax
import jax.numpy as jnp
from jax import lax
from jax.sharding import PartitionSpec as P

CHUNKS = 2
GROUP = ("gr", "tp")


def normalize(rows_in):
    values = rows_in.astype(jnp.float32)
    scaled = values * lax.rsqrt(jnp.mean(values * values, axis=-1, keepdims=True) + 1e-06)
    return scaled.astype(jnp.bfloat16)


def mixing(chosen, weights, experts):
    share = weights / jnp.sum(weights, axis=-1, keepdims=True)
    labels = jnp.arange(experts, dtype=jnp.int32)
    match = (chosen[:, :, None] == labels[None, None, :]).astype(jnp.float32)
    return jnp.sum(share[:, :, None] * match, axis=1)


def expert_term(normed, mix_column, gate_weight, up_weight, down_weight):
    gate_act = jnp.dot(normed, gate_weight, preferred_element_type=jnp.float32)
    up_act = jnp.dot(normed, up_weight, preferred_element_type=jnp.float32)
    hidden = (jax.nn.silu(gate_act) * up_act).astype(jnp.bfloat16)
    projected = jnp.dot(hidden, down_weight, preferred_element_type=jnp.float32)
    return mix_column * projected


def make_shards(n_fs, n_group):
    def by_chunks(rows):
        parts = rows.reshape(n_fs, CHUNKS, -1, rows.shape[-1])
        return parts.transpose(1, 0, 2, 3).reshape(rows.shape)

    def shards(tokens, gate_master, up_master, down_master, norm_gain, route, route_weight):
        experts, depth, columns = gate_master.shape
        blocks = n_fs // n_group
        width = columns // blocks
        rows = depth // n_group

        down_local = down_master.astype(jnp.bfloat16)
        down_local, gate_master, up_master = lax.optimization_barrier((down_local, gate_master, up_master))
        down_list = [lax.all_gather(down_local[index], GROUP, axis=1, tiled=True) for index in range(experts)]

        def local(master, index):
            scaled = (norm_gain[:, None] * master[index]).astype(jnp.bfloat16)
            return scaled.reshape(n_group, rows, blocks, width).transpose(0, 2, 1, 3)

        me = lax.axis_index("fs")

        def permuted(sent):
            got = [lax.dynamic_index_in_dim(sent, me, 0, keepdims=True)]
            for shift in range(1, n_fs):
                block = lax.dynamic_index_in_dim(sent, lax.rem(me + shift, n_fs), 0, keepdims=True)
                got.append(lax.ppermute(block, "fs", [(i, (i + shift) % n_fs) for i in range(n_fs)]))
            return got

        def gathered(got):
            mine = jnp.zeros((n_fs,) + got[0].shape[1:], got[0].dtype)
            for shift in range(n_fs):
                source = lax.rem(me - shift + n_fs, n_fs)
                mine = lax.dynamic_update_slice_in_dim(mine, got[shift], source, 0)
            return tuple(
                lax.all_gather(mine[:, which], GROUP, axis=1, tiled=True).reshape(n_fs * depth, width)
                for which in range(2)
            )

        pair = jnp.stack([local(m, i) for i in range(experts) for m in (gate_master, up_master)], axis=2)
        pair = lax.all_to_all(pair, GROUP, split_axis=0, concat_axis=0, tiled=True)
        pair = pair.reshape(n_fs, 2 * experts, rows, width)

        got = [permuted(pair[:, 2 * index : 2 * index + 2]) for index in range(experts)]
        got[0], down_list = lax.optimization_barrier((got[0], down_list))

        normed = by_chunks(normalize(tokens[0]))
        combine = by_chunks(mixing(route[0], route_weight[0], experts))
        total = jnp.zeros(normed.shape, jnp.float32)
        weights = [gathered(got[index]) for index in range(min(2, experts))]
        for index in range(experts - 1):
            total = total + expert_term(
                normed, combine[:, index : index + 1], *weights[index], down_list[index]
            )
            if index + 2 < experts:
                got[index + 2], total = lax.optimization_barrier((got[index + 2], total))
                weights.append(gathered(got[index + 2]))
        last = experts - 1
        size = normed.shape[0] // CHUNKS
        mixed = []
        for chunk in range(CHUNKS):
            part = slice(chunk * size, (chunk + 1) * size)
            summed = total[part] + expert_term(
                normed[part], combine[part, last : last + 1], *weights[last], down_list[last]
            )
            summed = summed.astype(jnp.bfloat16)
            mixed.append(lax.psum_scatter(summed, "fs", scatter_dimension=0, tiled=True))
        weights, down_list, _ = lax.optimization_barrier((weights, down_list, summed))
        gate_out = jnp.stack([pair[0] for pair in weights], axis=0)
        up_out = jnp.stack([pair[1] for pair in weights], axis=0)
        down_out = jnp.stack(down_list, axis=0)
        return (gate_out, up_out, down_out, jnp.concatenate(mixed, axis=0)[None])

    return shards


def solution(mesh):
    n_fs = mesh.shape["fs"]
    n_group = mesh.shape["gr"] * mesh.shape["tp"]
    in_specs = (
        P(GROUP, None, None),
        P(None, "fs", GROUP),
        P(None, "fs", GROUP),
        P(None, "fs", GROUP),
        P("fs"),
        P(GROUP, None, None),
        P(GROUP, None, None),
    )
    out_specs = (
        P(None, None, "fs"),
        P(None, None, "fs"),
        P(None, "fs", None),
        P(GROUP, "fs", None),
    )
    return jax.shard_map(
        make_shards(n_fs, n_group), mesh=mesh, in_specs=in_specs, out_specs=out_specs, check_vma=False
    )
```

time: 767 us -> 623 us (0.81)
  waiting for transfers between devices: 506 us -> 266 us
  other arithmetic: 42.6 us -> 74 us
  starting transfers between devices: 40.6 us -> 65.8 us
  local copies, waits for them, and re-layouts: 36.1 us -> 57.7 us
  matrix products: 125 us -> 135 us
    all_to_all x6 -> x1, waiting for transfers between devices: 332 us -> 99.7 us  [shards(): pair = lax.all_to_all(pair, GROUP, split_axis=0, concat_axis=0, tiled=True)]
    ppermute x0 -> x21, starting transfers between devices: none -> 59.3 us  [permuted(): lax.ppermute(block, 'fs', [(i, (i + shift) % n_fs) for i in range(n_fs)])]
    all_gather x9, waiting for transfers between devices: 53.8 us -> 0.05 us  [the longest x6 0.04 us: gathered(): lax.all_gather(mine[:, which], GROUP, axis=1, tiled=True)]
    ppermute x0 -> x21, waiting for transfers between devices: none -> 37.3 us  [permuted(): lax.ppermute(block, 'fs', [(i, (i + shift) % n_fs) for i in range(n_fs)])]
    all_to_all x6 -> x1, starting transfers between devices: 40.2 us -> 5.22 us  [shards(): pair = lax.all_to_all(pair, GROUP, split_axis=0, concat_axis=0, tiled=True)]
    add x0 -> x1, other arithmetic: none -> 19.1 us  [shards(): total + expert_term(normed, combine[:, index:index + 1], *weights[index],...]
    slice x2 -> x7, local copies, waits for them, and re-layouts: 3.17 us -> 20.1 us  [the longest x1 7.93 us: local(): scaled = (norm_gain[:, None] * master[index]).astype(jnp.bfloat16)]
    squeeze x0 -> x6, local copies, waits for them, and re-layouts: none -> 16.6 us  [local(): scaled = (norm_gain[:, None] * master[index]).astype(jnp.bfloat16)]
  transfers between devices with their start and end apart: 16 -> 33, of which waited for: 9 -> 12; matrix products, arithmetic and copies ran while one was open for 22% -> 39% of each run, Pallas kernels for 0% -> 0%
where the time goes in v1:
time: 623 us; the launch traced here: 614 us
  waiting for transfers between devices  266 us (43%)
  matrix products  135 us (22%)
  other arithmetic  74 us (12%)
  starting transfers between devices  65.8 us (11%)
  local copies, waits for them, and re-layouts  57.7 us (9%)
  between operations  14.8 us (2%)
    reduce_scatter x2, waiting for transfers between devices, shards(): lax.psum_scatter(summed, 'fs', scatter_dimension=0, tiled=True)  127 us
    all_to_all x1, waiting for transfers between devices, shards(): pair = lax.all_to_all(pair, GROUP, split_axis=0, concat_axis=0, tiled=True)  99.7 us
    dot_general x4, matrix products, expert_term(): projected = jnp.dot(hidden, down_weight, preferred_element_type=jnp.float32)  87.4 us
    ppermute x21, starting transfers between devices, permuted(): lax.ppermute(block, 'fs', [(i, (i + shift) % n_fs) for i in range(n_fs)])  59.3 us
    dot_general x4, matrix products, expert_term(): gate_act = jnp.dot(normed, gate_weight, preferred_element_type=jnp.float32)  47.6 us
    ppermute x21, waiting for transfers between devices, permuted(): lax.ppermute(block, 'fs', [(i, (i + shift) % n_fs) for i in range(n_fs)])  37.3 us
    add x1, other arithmetic, shards(): total + expert_term(normed, combine[:, index:index + 1], *weights[index],...  19.1 us
    squeeze x6, local copies, waits for them, and re-layouts, local(): scaled = (norm_gain[:, None] * master[index]).astype(jnp.bfloat16)  16.6 us
  transfers between devices with their start and end apart: 33, of which 12 were waited for; matrix products, arithmetic and copies ran while one was open for 39% of the time, Pallas kernels for 0%

profile of v1, /device:TPU:0, one launch (start us, length us, event | category | flops | bytes accessed | tf_op | source)
XLA Modules:
  0.0 613.7 jit_solution(14788001675067907595)
XLA Ops:
  13.2 7.9 %fusion.25 = (f32[1,256,1792]{2,1,0:T(8,128)}, f32[1,256,1792]{2,1,0:T(8,128)S(1)}, f32[1,256,1792]{2,1,0:T(8,128)}, f32[1,256,1792]{2,1,0:T(8,128)}, f32[1,256,1792]{2,1,0:T(8,128)}, /*index=5*/f32[1,256,1792]{2,1,0:T(8,128)}) fusion(f32[3,256,1792]{2,1,0:T(8,128)} %param.9, f32[3,256,1792]{2,1,0:T(8,128)} %param.8), kind=kLoop, calls=%fused_computation.97 | loop fusion | bytes 22020096 | tf_op jit(solution)/shard_map/slice | solution.py:47
  21.2 3.3 squeeze.49
  50.9 5.2 all-to-all-start
  56.7 99.7 %all-to-all-done = bf16[4,2,6,64,896]{4,1,3,2,0:T(2,128)(2,1)} async-done(((bf16[4,2,6,64,896]{4,1,3,2,0:T(2,128)(2,1)}), bf16[4,2,6,64,896]{4,1,3,2,0:T(2,128)(2,1)}, u32[]{:S(2)}, u32[]{:S(2)}) %all-to-all-start) | async-done | bytes 5505056 | tf_op jit(solution)/shard_map/all_to_all | solution.py:70
  156.3 3.7 copy.48
  175.6 4.2 collective-permute-start.6
  179.8 12.9 %collective-permute-done.2 = bf16[1,2,64,896]{3,2,1,0:T(8,128)(2,1)S(1)} collective-permute-done((bf16[1,2,64,896]{3,2,1,0:T(8,128)(2,1)}, bf16[1,2,64,896]{3,2,1,0:T(8,128)(2,1)S(1)}, u32[]{:S(2)}, u32[]{:S(2)}) %collective-permute-start.2) | collective-permute-done | bytes 229408 | tf_op jit(solution)/shard_map/ppermute | solution.py:56
  199.3 4.4 collective-permute-start.7
  203.7 10.3 %collective-permute-start.8 = (bf16[1,2,64,896]{3,2,1,0:T(8,128)(2,1)S(1)}, bf16[1,2,64,896]{3,2,1,0:T(8,128)(2,1)S(1)}, u32[]{:S(2)}, u32[]{:S(2)}) collective-permute-start(bf16[1,2,64,896]{3,2,1,0:T(8,128)(2,1)S(1)} %get-tuple-element.99), channel_id=1, source_target_pairs={{0,4},{2,6},{4,8},{6,10},{8,12},{10,14},{12,0},{14,2},{1,5},{3,7},... | collective-permute-start | bytes 688136 | tf_op jit(solution)/shard_map/ppermute | solution.py:56
  221.0 4.3 collective-permute-start.13
  225.4 13.4 %collective-permute-done.9 = bf16[1,2,64,896]{3,2,1,0:T(8,128)(2,1)S(1)} collective-permute-done((bf16[1,2,64,896]{3,2,1,0:T(8,128)(2,1)S(1)}, bf16[1,2,64,896]{3,2,1,0:T(8,128)(2,1)S(1)}, u32[]{:S(2)}, u32[]{:S(2)}) %collective-permute-start.9) | collective-permute-done | bytes 229408 | tf_op jit(solution)/shard_map/ppermute | solution.py:56
  239.8 3.7 collective-permute-done.13
  244.9 5.1 multiply_reduce_fusion
  250.0 8.8 %fusion = bf16[2,8,128,2048]{3,2,0,1:T(8,128)(2,1)} fusion(f32[8,2,128]{2,1,0:T(2,128)S(1)} %bitcast.148, bf16[8,2,128,2048]{3,2,1,0:T(8,128)(2,1)} %bitcast.116), kind=kLoop, calls=%fused_computation.7 | loop fusion | flops 12582912 | bytes 16785408 | tf_op jit(solution)/shard_map/transpose | solution.py:34
  258.9 8.6 %copy.50 = bf16[2,8,128,2048]{3,2,1,0:T(8,128)(2,1)} copy(bf16[2,8,128,2048]{3,2,0,1:T(8,128)(2,1)} %fusion) | data formatting | bytes 16777216 | tf_op jit(solution)/shard_map/transpose | solution.py:34
  270.7 9.7 %collective-permute-start.15 = (bf16[1,2,64,896]{3,2,1,0:T(8,128)(2,1)S(1)}, bf16[1,2,64,896]{3,2,1,0:T(8,128)(2,1)S(1)}, u32[]{:S(2)}, u32[]{:S(2)}) collective-permute-start(bf16[1,2,64,896]{3,2,1,0:T(8,128)(2,1)S(1)} %get-tuple-element.89), channel_id=1, source_target_pairs={{0,4},{2,6},{4,8},{6,10},{8,12},{10,14},{12,0},{14,2},{1,5},{3,7},... | collective-permute-start | bytes 688136 | tf_op jit(solution)/shard_map/ppermute | solution.py:56
  280.4 3.5 collective-permute-start.17
  287.2 14.2 %fusion.33 = f32[2048,896]{1,0:T(8,128)} fusion(bf16[2048,2048]{1,0:T(8,128)(2,1)} %bitcast.118, bf16[2048,896]{1,0:T(8,128)(2,1)} %bitcast.130), kind=kOutput, calls=%fused_computation.105 | convolution fusion | flops 7516192768 | bytes 19398656 | tf_op jit(solution)/shard_map/dot_general | solution.py:24
  303.3 26.8 %convolution_multiply_fusion = f32[2048,2048]{1,0:T(8,128)} fusion(bf16[896,2048]{1,0:T(8,128)(2,1)} %bitcast.126, f32[2048]{0:T(1024)S(1)} %bitcast.151, f32[2048,896]{1,0:T(8,128)} %fusion.33, bf16[2048,2048]{1,0:T(8,128)(2,1)} %bitcast.119, bf16[2048,896]{1,0:T(8,128)(2,1)} %bitcast.132), kind=kOutput, calls=%fused_computation.6 | convolution fusion | flops 15047589888 | bytes 39854080 | tf_op jit(solution)/shard_map/dot_general | solution.py:27
  332.6 6.2 %fusion.23 = (bf16[1,8,128,2048]{3,2,0,1:T(8,128)(2,1)}, bf16[1,8,128,2048]{3,2,0,1:T(8,128)(2,1)}) fusion(bf16[2,8,128,2048]{3,2,0,1:T(8,128)(2,1)} %fusion), kind=kLoop, calls=%fused_computation.95 | loop fusion | bytes 16777216 | tf_op jit(solution)/shard_map/slice | solution.py:93
  338.8 14.2 %fusion.34 = f32[2048,896]{1,0:T(8,128)} fusion(bf16[2048,2048]{1,0:T(8,128)(2,1)} %bitcast.120, bf16[2048,896]{1,0:T(8,128)(2,1)} %bitcast.134), kind=kOutput, calls=%fused_computation.106 | convolution fusion | flops 7516192768 | bytes 19398656 | tf_op jit(solution)/shard_map/dot_general | solution.py:24
  353.0 26.7 %fusion.3 = f32[2048,2048]{1,0:T(8,128)} fusion(bf16[896,2048]{1,0:T(8,128)(2,1)} %bitcast.127, f32[2048,896]{1,0:T(8,128)} %fusion.34, bf16[2048,2048]{1,0:T(8,128)(2,1)} %bitcast.121, bf16[2048,896]{1,0:T(8,128)(2,1)} %bitcast.136), kind=kOutput, calls=%fused_computation.14 | convolution fusion | flops 15043395584 | bytes 39845888 | tf_op jit(solution)/shard_map/dot_general | solution.py:27
  379.8 19.1 %multiply_add_fusion = f32[2048,2048]{1,0:T(8,128)} fusion(f32[2048,2048]{1,0:T(8,128)} %convolution_multiply_fusion, f32[2048,2048]{1,0:T(8,128)} %fusion.3, f32[2048]{0:T(1024)S(1)} %bitcast.149), kind=kLoop, calls=%fused_computation | loop fusion | flops 8388608 | bytes 50339840 | tf_op jit(solution)/shard_map/add | solution.py:81
  398.8 9.6 %fusion.36 = f32[1024,896]{1,0:T(8,128)} fusion(bf16[1024,2048]{1,0:T(8,128)(2,1)} %bitcast.124, bf16[2048,896]{1,0:T(8,128)(2,1)} %bitcast.138), kind=kOutput, calls=%fused_computation.108 | convolution fusion | flops 3758096384 | bytes 11534336 | tf_op jit(solution)/shard_map/dot_general | solution.py:24
  408.5 17.3 %fusion.1 = bf16[1024,2048]{1,0:T(8,128)(2,1)} fusion(f32[2048,2048]{1,0:T(8,128)} %multiply_add_fusion, bf16[896,2048]{1,0:T(8,128)(2,1)} %bitcast.128, f32[1024]{0:T(1024)S(1)} %bitcast.153, f32[1024,896]{1,0:T(8,128)} %fusion.36, bf16[1024,2048]{1,0:T(8,128)(2,1)} %bitcast.125, bf16[2048,896]{1,0:T(8,128)(2,1)} %bitcast.141), kind=kOutput, calls=%fused_computation.9 | convolution fusion | flops 7527989248 | bytes 27791360 | tf_op jit(solution)/shard_map/dot_general | solution.py:27
  425.9 9.6 %fusion.35 = f32[1024,896]{1,0:T(8,128)} fusion(bf16[1024,2048]{1,0:T(8,128)(2,1)} %bitcast.122, bf16[2048,896]{1,0:T(8,128)(2,1)} %bitcast.139), kind=kOutput, calls=%fused_computation.107 | convolution fusion | flops 3758096384 | bytes 11534336 | tf_op jit(solution)/shard_map/dot_general | solution.py:24
  435.5 16.6 %fusion.2 = bf16[1024,2048]{1,0:T(8,128)(2,1)} fusion(f32[2048,2048]{1,0:T(8,128)} %multiply_add_fusion, bf16[896,2048]{1,0:T(8,128)(2,1)} %bitcast.129, f32[1024]{0:T(1024)S(1)} %bitcast.152, f32[1024,896]{1,0:T(8,128)} %fusion.35, bf16[1024,2048]{1,0:T(8,128)(2,1)} %bitcast.123, bf16[2048,896]{1,0:T(8,128)(2,1)} %bitcast.142), kind=kOutput, calls=%fused_computation.11 | convolution fusion | flops 7527989248 | bytes 27791360 | tf_op jit(solution)/shard_map/dot_general | solution.py:27
  452.1 11.9 %pad_maximum_fusion.2 = bf16[3,896,2048]{2,1,0:T(8,128)(2,1)} fusion(bf16[1,896,2048]{2,1,0:T(8,128)(2,1)} %all-gather.23.cloned.1.call-done, bf16[1,896,2048]{2,1,0:T(8,128)(2,1)} %all-gather.21.cloned.1.call-done, bf16[1,896,2048]{2,1,0:T(8,128)(2,1)} %all-gather.19.cloned.1.call-done), kind=kLoop, calls=%fused_computation.5 | loop fusion | flops 11010048 | bytes 22020096 | tf_op jit(solution)/shard_map/stack | solution.py:100
  464.1 5.8 pad_maximum_fusion.1
  472.1 5.0 pad_maximum_fusion
  477.1 35.7 %reduce-scatter.3.cloned.1.call-done = bf16[128,2048]{1,0:T(8,128)(2,1)} async-done(((bf16[1024,2048]{1,0:T(8,128)(2,1)}), bf16[128,2048]{1,0:T(8,128)(2,1)}) %reduce-scatter.3.cloned.1.call-update) | async-done | bytes 524304 | tf_op jit(solution)/shard_map/reduce_scatter | solution.py:96
  512.8 91.6 %reduce-scatter.5.cloned.1.call-done = bf16[128,2048]{1,0:T(8,128)(2,1)} async-done(((bf16[1024,2048]{1,0:T(8,128)(2,1)}), bf16[128,2048]{1,0:T(8,128)(2,1)}) %reduce-scatter.5.cloned.1.call-update) | async-done | bytes 524304 | tf_op jit(solution)/shard_map/reduce_scatter | solution.py:96
  (146 shorter events, 79.8 us)
Async XLA Ops:
  7.2 188.1 %all-gather.19.cloned.1.call-start = ((), (), s32[]{:S(2)}) async-start(), calls=%async_computation.5 | async-start | bytes 4587520 | tf_op jit(solution)/shard_map/all_gather | solution.py:44
  11.7 183.5 %all-gather.21.cloned.1.call-start = ((), (), s32[]{:S(2)}) async-start(), calls=%async_computation.6 | async-start | bytes 4587520 | tf_op jit(solution)/shard_map/all_gather | solution.py:44
  12.5 182.8 %all-gather.23.cloned.1.call-start = ((), (), s32[]{:S(2)}) async-start(), calls=%async_computation.7 | async-start | bytes 4587520 | tf_op jit(solution)/shard_map/all_gather | solution.py:44
  50.9 105.5 %all-to-all-start = ((bf16[4,2,6,64,896]{4,1,3,2,0:T(2,128)(2,1)}), bf16[4,2,6,64,896]{4,1,3,2,0:T(2,128)(2,1)}, u32[]{:S(2)}, u32[]{:S(2)}) async-start(bf16[4,2,6,64,896]{4,1,3,2,0:T(2,128)(2,1)} %fusion.17), calls=%async_computation | async-start | bytes 11010048 | tf_op jit(solution)/shard_map/all_to_all | solution.py:70
  56.1 231.1 %all-gather.25.cloned.1.call-start = ((), (), s32[]{:S(2)}) async-start(), calls=%async_computation.8 | async-start | bytes 4587520 | tf_op jit(solution)/shard_map/all_gather | solution.py:65
  162.9 11.4 %collective-permute-start = (bf16[1,2,64,896]{3,2,1,0:T(8,128)(2,1)S(1)}, bf16[1,2,64,896]{3,2,1,0:T(8,128)(2,1)S(1)}, u32[]{:S(2)}, u32[]{:S(2)}) collective-permute-start(bf16[1,2,64,896]{3,2,1,0:T(8,128)(2,1)S(1)} %get-tuple-element.110), channel_id=1, source_target_pairs={{0,2},{2,4},{4,6},{6,8},{8,10},{10,12},{12,14},{14,0},{1,3},{3,5},... | collective-permute-start | bytes 688136 | tf_op jit(solution)/shard_map/ppermute | solution.py:56
  165.8 26.9 %collective-permute-start.2 = (bf16[1,2,64,896]{3,2,1,0:T(8,128)(2,1)}, bf16[1,2,64,896]{3,2,1,0:T(8,128)(2,1)S(1)}, u32[]{:S(2)}, u32[]{:S(2)}) collective-permute-start(bf16[1,2,64,896]{3,2,1,0:T(8,128)(2,1)} %get-tuple-element.108), channel_id=1, source_target_pairs={{0,6},{2,8},{4,10},{6,12},{8,14},{10,0},{12,2},{14,4},{1,7},{3,9},... | collective-permute-start | bytes 688136 | tf_op jit(solution)/shard_map/ppermute | solution.py:56
  168.2 24.9 %collective-permute-start.3 = (bf16[1,2,64,896]{3,2,1,0:T(8,128)(2,1)}, bf16[1,2,64,896]{3,2,1,0:T(8,128)(2,1)S(1)}, u32[]{:S(2)}, u32[]{:S(2)}) collective-permute-start(bf16[1,2,64,896]{3,2,1,0:T(8,128)(2,1)} %get-tuple-element.107), channel_id=1, source_target_pairs={{0,8},{2,10},{4,12},{6,14},{8,0},{10,2},{12,4},{14,6},{1,9},{3,11}... | collective-permute-start | bytes 688136 | tf_op jit(solution)/shard_map/ppermute | solution.py:56
  169.6 23.5 %collective-permute-start.4 = (bf16[1,2,64,896]{3,2,1,0:T(8,128)(2,1)}, bf16[1,2,64,896]{3,2,1,0:T(8,128)(2,1)S(1)}, u32[]{:S(2)}, u32[]{:S(2)}) collective-permute-start(bf16[1,2,64,896]{3,2,1,0:T(8,128)(2,1)} %get-tuple-element.106), channel_id=1, source_target_pairs={{0,10},{2,12},{4,14},{6,0},{8,2},{10,4},{12,6},{14,8},{1,11},{3,13... | collective-permute-start | bytes 688136 | tf_op jit(solution)/shard_map/ppermute | solution.py:56
  174.2 18.9 %collective-permute-start.5 = (bf16[1,2,64,896]{3,2,1,0:T(8,128)(2,1)}, bf16[1,2,64,896]{3,2,1,0:T(8,128)(2,1)S(1)}, u32[]{:S(2)}, u32[]{:S(2)}) collective-permute-start(bf16[1,2,64,896]{3,2,1,0:T(8,128)(2,1)} %get-tuple-element.105), channel_id=1, source_target_pairs={{0,12},{2,14},{4,0},{6,2},{8,4},{10,6},{12,8},{14,10},{1,13},{3,15... | collective-permute-start | bytes 688136 | tf_op jit(solution)/shard_map/ppermute | solution.py:56
  175.6 19.7 %collective-permute-start.6 = (bf16[1,2,64,896]{3,2,1,0:T(8,128)(2,1)}, bf16[1,2,64,896]{3,2,1,0:T(8,128)(2,1)}, u32[]{:S(2)}, u32[]{:S(2)}) collective-permute-start(bf16[1,2,64,896]{3,2,1,0:T(8,128)(2,1)} %get-tuple-element.104), channel_id=1, source_target_pairs={{0,14},{2,0},{4,2},{6,4},{8,6},{10,8},{12,10},{14,12},{1,15},{3,1}... | collective-permute-start | bytes 688136 | tf_op jit(solution)/shard_map/ppermute | solution.py:56
  198.2 105.1 %all-gather.27.cloned.1.call-start = ((), (), s32[]{:S(2)}) async-start(), calls=%async_computation.9 | async-start | bytes 4587520 | tf_op jit(solution)/shard_map/all_gather | solution.py:65
  198.8 140.0 %all-gather.29.cloned.1.call-start = ((), (), s32[]{:S(2)}) async-start(), calls=%async_computation.10 | async-start | bytes 4587520 | tf_op jit(solution)/shard_map/all_gather | solution.py:65
  199.3 21.7 %collective-permute-start.7 = (bf16[1,2,64,896]{3,2,1,0:T(8,128)(2,1)S(1)}, bf16[1,2,64,896]{3,2,1,0:T(8,128)(2,1)S(1)}, u32[]{:S(2)}, u32[]{:S(2)}) collective-permute-start(bf16[1,2,64,896]{3,2,1,0:T(8,128)(2,1)S(1)} %get-tuple-element.100), channel_id=1, source_target_pairs={{0,2},{2,4},{4,6},{6,8},{8,10},{10,12},{12,14},{14,0},{1,3},{3,5},... | collective-permute-start | bytes 688136 | tf_op jit(solution)/shard_map/ppermute | solution.py:56
  203.7 17.3 %collective-permute-start.8 = (bf16[1,2,64,896]{3,2,1,0:T(8,128)(2,1)S(1)}, bf16[1,2,64,896]{3,2,1,0:T(8,128)(2,1)S(1)}, u32[]{:S(2)}, u32[]{:S(2)}) collective-permute-start(bf16[1,2,64,896]{3,2,1,0:T(8,128)(2,1)S(1)} %get-tuple-element.99), channel_id=1, source_target_pairs={{0,4},{2,6},{4,8},{6,10},{8,12},{10,14},{12,0},{14,2},{1,5},{3,7},... | collective-permute-start | bytes 688136 | tf_op jit(solution)/shard_map/ppermute | solution.py:56
  214.0 24.7 %collective-permute-start.9 = (bf16[1,2,64,896]{3,2,1,0:T(8,128)(2,1)S(1)}, bf16[1,2,64,896]{3,2,1,0:T(8,128)(2,1)S(1)}, u32[]{:S(2)}, u32[]{:S(2)}) collective-permute-start(bf16[1,2,64,896]{3,2,1,0:T(8,128)(2,1)S(1)} %get-tuple-element.98), channel_id=1, source_target_pairs={{0,6},{2,8},{4,10},{6,12},{8,14},{10,0},{12,2},{14,4},{1,7},{3,9},... | collective-permute-start | bytes 688136 | tf_op jit(solution)/shard_map/ppermute | solution.py:56
  214.0 25.0 %collective-permute-start.10 = (bf16[1,2,64,896]{3,2,1,0:T(8,128)(2,1)S(1)}, bf16[1,2,64,896]{3,2,1,0:T(8,128)(2,1)S(1)}, u32[]{:S(2)}, u32[]{:S(2)}) collective-permute-start(bf16[1,2,64,896]{3,2,1,0:T(8,128)(2,1)S(1)} %get-tuple-element.97), channel_id=1, source_target_pairs={{0,8},{2,10},{4,12},{6,14},{8,0},{10,2},{12,4},{14,6},{1,9},{3,11}... | collective-permute-start | bytes 688136 | tf_op jit(solution)/shard_map/ppermute | solution.py:56
  216.0 23.1 %collective-permute-start.11 = (bf16[1,2,64,896]{3,2,1,0:T(8,128)(2,1)S(1)}, bf16[1,2,64,896]{3,2,1,0:T(8,128)(2,1)S(1)}, u32[]{:S(2)}, u32[]{:S(2)}) collective-permute-start(bf16[1,2,64,896]{3,2,1,0:T(8,128)(2,1)S(1)} %get-tuple-element.96), channel_id=1, source_target_pairs={{0,10},{2,12},{4,14},{6,0},{8,2},{10,4},{12,6},{14,8},{1,11},{3,13... | collective-permute-start | bytes 688136 | tf_op jit(solution)/shard_map/ppermute | solution.py:56
  221.0 18.7 %collective-permute-start.12 = (bf16[1,2,64,896]{3,2,1,0:T(8,128)(2,1)S(1)}, bf16[1,2,64,896]{3,2,1,0:T(8,128)(2,1)S(1)}, u32[]{:S(2)}, u32[]{:S(2)}) collective-permute-start(bf16[1,2,64,896]{3,2,1,0:T(8,128)(2,1)S(1)} %get-tuple-element.95), channel_id=1, source_target_pairs={{0,12},{2,14},{4,0},{6,2},{8,4},{10,6},{12,8},{14,10},{1,13},{3,15... | collective-permute-start | bytes 688136 | tf_op jit(solution)/shard_map/ppermute | solution.py:56
  221.0 22.4 %collective-permute-start.13 = (bf16[1,2,64,896]{3,2,1,0:T(8,128)(2,1)S(1)}, bf16[1,2,64,896]{3,2,1,0:T(8,128)(2,1)S(1)}, u32[]{:S(2)}, u32[]{:S(2)}) collective-permute-start(bf16[1,2,64,896]{3,2,1,0:T(8,128)(2,1)S(1)} %get-tuple-element.94), channel_id=1, source_target_pairs={{0,14},{2,0},{4,2},{6,4},{8,6},{10,8},{12,10},{14,12},{1,15},{3,1}... | collective-permute-start | bytes 688136 | tf_op jit(solution)/shard_map/ppermute | solution.py:56
  244.9 108.1 %all-gather.31.cloned.1.call-start = ((), (), s32[]{:S(2)}) async-start(), calls=%async_computation.11 | async-start | bytes 4587520 | tf_op jit(solution)/shard_map/all_gather | solution.py:65
  268.7 32.7 %collective-permute-start.14 = (bf16[1,2,64,896]{3,2,1,0:T(8,128)(2,1)}, bf16[1,2,64,896]{3,2,1,0:T(8,128)(2,1)S(1)}, u32[]{:S(2)}, u32[]{:S(2)}) collective-permute-start(bf16[1,2,64,896]{3,2,1,0:T(8,128)(2,1)} %get-tuple-element.90), channel_id=1, source_target_pairs={{0,2},{2,4},{4,6},{6,8},{8,10},{10,12},{12,14},{14,0},{1,3},{3,5},... | collective-permute-start | bytes 688136 | tf_op jit(solution)/shard_map/ppermute | solution.py:56
  270.7 30.9 %collective-permute-start.15 = (bf16[1,2,64,896]{3,2,1,0:T(8,128)(2,1)S(1)}, bf16[1,2,64,896]{3,2,1,0:T(8,128)(2,1)S(1)}, u32[]{:S(2)}, u32[]{:S(2)}) collective-permute-start(bf16[1,2,64,896]{3,2,1,0:T(8,128)(2,1)S(1)} %get-tuple-element.89), channel_id=1, source_target_pairs={{0,4},{2,6},{4,8},{6,10},{8,12},{10,14},{12,0},{14,2},{1,5},{3,7},... | collective-permute-start | bytes 688136 | tf_op jit(solution)/shard_map/ppermute | solution.py:56
  280.4 49.8 %collective-permute-start.16 = (bf16[1,2,64,896]{3,2,1,0:T(8,128)(2,1)S(1)}, bf16[1,2,64,896]{3,2,1,0:T(8,128)(2,1)S(1)}, u32[]{:S(2)}, u32[]{:S(2)}) collective-permute-start(bf16[1,2,64,896]{3,2,1,0:T(8,128)(2,1)S(1)} %get-tuple-element.88), channel_id=1, source_target_pairs={{0,6},{2,8},{4,10},{6,12},{8,14},{10,0},{12,2},{14,4},{1,7},{3,9},... | collective-permute-start | bytes 688136 | tf_op jit(solution)/shard_map/ppermute | solution.py:56
  280.4 49.8 %collective-permute-start.17 = (bf16[1,2,64,896]{3,2,1,0:T(8,128)(2,1)S(1)}, bf16[1,2,64,896]{3,2,1,0:T(8,128)(2,1)S(1)}, u32[]{:S(2)}, u32[]{:S(2)}) collective-permute-start(bf16[1,2,64,896]{3,2,1,0:T(8,128)(2,1)S(1)} %get-tuple-element.87), channel_id=1, source_target_pairs={{0,8},{2,10},{4,12},{6,14},{8,0},{10,2},{12,4},{14,6},{1,9},{3,11}... | collective-permute-start | bytes 688136 | tf_op jit(solution)/shard_map/ppermute | solution.py:56
  283.9 46.2 %collective-permute-start.18 = (bf16[1,2,64,896]{3,2,1,0:T(8,128)(2,1)S(1)}, bf16[1,2,64,896]{3,2,1,0:T(8,128)(2,1)S(1)}, u32[]{:S(2)}, u32[]{:S(2)}) collective-permute-start(bf16[1,2,64,896]{3,2,1,0:T(8,128)(2,1)S(1)} %get-tuple-element.86), channel_id=1, source_target_pairs={{0,10},{2,12},{4,14},{6,0},{8,2},{10,4},{12,6},{14,8},{1,11},{3,13... | collective-permute-start | bytes 688136 | tf_op jit(solution)/shard_map/ppermute | solution.py:56
  286.9 111.9 %all-gather.33.cloned.1.call-start = ((), (), s32[]{:S(2)}) async-start(), calls=%async_computation.12 | async-start | bytes 4587520 | tf_op jit(solution)/shard_map/all_gather | solution.py:65
  301.4 28.8 %collective-permute-start.19 = (bf16[1,2,64,896]{3,2,1,0:T(8,128)(2,1)S(1)}, bf16[1,2,64,896]{3,2,1,0:T(8,128)(2,1)S(1)}, u32[]{:S(2)}, u32[]{:S(2)}) collective-permute-start(bf16[1,2,64,896]{3,2,1,0:T(8,128)(2,1)S(1)} %get-tuple-element.85), channel_id=1, source_target_pairs={{0,12},{2,14},{4,0},{6,2},{8,4},{10,6},{12,8},{14,10},{1,13},{3,15... | collective-permute-start | bytes 688136 | tf_op jit(solution)/shard_map/ppermute | solution.py:56
  301.6 28.6 %collective-permute-start.20 = (bf16[1,2,64,896]{3,2,1,0:T(8,128)(2,1)S(1)}, bf16[1,2,64,896]{3,2,1,0:T(8,128)(2,1)S(1)}, u32[]{:S(2)}, u32[]{:S(2)}) collective-permute-start(bf16[1,2,64,896]{3,2,1,0:T(8,128)(2,1)S(1)} %get-tuple-element.84), channel_id=1, source_target_pairs={{0,14},{2,0},{4,2},{6,4},{8,6},{10,8},{12,10},{14,12},{1,15},{3,1}... | collective-permute-start | bytes 688136 | tf_op jit(solution)/shard_map/ppermute | solution.py:56
  332.3 76.2 %all-gather.35.cloned.1.call-start = ((), (), s32[]{:S(2)}) async-start(), calls=%async_computation.13 | async-start | bytes 4587520 | tf_op jit(solution)/shard_map/all_gather | solution.py:65
  353.0 159.8 %reduce-scatter.3.cloned.1.call-start = ((), (), s32[]{:S(2)}) async-start(), calls=%async_computation.3 | async-start | bytes 4718592 | tf_op jit(solution)/shard_map/reduce_scatter | solution.py:96
  425.8 178.6 %reduce-scatter.5.cloned.1.call-start = ((), (), s32[]{:S(2)}) async-start(), calls=%async_computation.4 | async-start | bytes 4718592 | tf_op jit(solution)/shard_map/reduce_scatter | solution.py:96
  (13 other events, 111.9 us)
Sparse Core Ops, SparseCore 0:
  11.9 34.1 all-gather.18
  47.7 49.1 all-gather.20
  99.0 50.1 all-gather.22
  198.3 42.3 all-gather.24
  242.7 31.4 all-gather.26
  275.6 31.4 all-gather.28
  308.7 31.4 all-gather.30
  341.8 31.4 all-gather.32
  375.4 31.4 all-gather.34
  425.9 86.7 reduce-scatter.2
  516.4 87.9 reduce-scatter.4
